TPU v7x, 512 devices: a whole 4x4x16 slice. The times are simulated.
512 devices in a mesh: sp: 32 (over z, core), tp: 16 (over y, x).
Axes of the slice: x: 4, y: 4, z: 16, core: 2. Of those that a mesh axis runs over, the one named last changes fastest.
Arguments:
- query_a: bfloat16 [6144, 2048], P('sp', 'tp'), may hold values from -6 to 6
- key_a: bfloat16 [6144, 2048], P('sp', 'tp'), may hold values from -6 to 6
- value_a: bfloat16 [6144, 2048], P('sp', 'tp'), may hold values from -6 to 6
- query_b: bfloat16 [6144, 2048], P('sp', 'tp'), may hold values from -6 to 6
- key_b: bfloat16 [6144, 2048], P('sp', 'tp'), may hold values from -6 to 6
- value_b: bfloat16 [6144, 2048], P('sp', 'tp'), may hold values from -6 to 6
- stop_a: float32 [6144, 32], P('sp', 'tp'), may hold values from -14 to -1
- stop_b: float32 [6144, 16], P('sp', 'tp'), may hold values from -14 to -1
- out_a: bfloat16 [2048, 2048], P('tp'), may hold values from -4 to 4
- out_b: bfloat16 [2048, 2048], P('tp'), may hold values from -4 to 4
- resid: bfloat16 [6144, 2048], P('sp', 'tp'), may hold values from -20 to 20
- mix_gain: float32 [2048], P('tp'), may hold values from 0.1 to 1.9
- ffn_gain: float32 [2048], P('tp'), may hold values from 0.1 to 1.9
- routes: int32 [6144, 2], P('sp'), may hold values from 0 to 127, all different within a row; in each aligned block of 192 rows (0 to 191, 192 to 383, ...) at most 5 rows name the same one
- gates: float32 [6144, 2], P('sp'), may hold values from 0.25 to 1.5
- exp_gate: bfloat16 [128, 2048, 512], P('sp', 'tp'), may hold values from -0.125 to 0.125
- exp_up: bfloat16 [128, 2048, 512], P('sp', 'tp'), may hold values from -0.125 to 0.125
- exp_down: bfloat16 [128, 512, 2048], P('sp', None, 'tp'), may hold values from -0.25 to 0.25
- sh_gate: bfloat16 [2048, 512], P('tp'), may hold values from -0.125 to 0.125
- sh_up: bfloat16 [2048, 512], P('tp'), may hold values from -0.125 to 0.125
- sh_down: bfloat16 [512, 2048], P(None, 'tp'), may hold values from -4 to 4
Outputs:
- result: bfloat16 [6144, 2048], P('sp', 'tp')
Inputs may be any that keep to these rules, and one draw needn't show every extreme that they name: `routes`: each row names 2 different experts. Within the rows of one index of sp (aligned blocks of 192 rows) no expert is named by more than 5 rows, a bound that some block reaches.
All inputs are finite; a program needn't handle non-finite values.
Results may differ from a plain program's by a relative error of at most 0.02.
Values may be sent and summed in bfloat16 or wider, within the bound.
A program may use at most 64 MiB of HBM per device.

v0:
```python
import jax
import jax.numpy as jnp
from jax import lax
from jax.sharding import Mesh
from jax.sharding import PartitionSpec as P

D = 2048
TP = ("tp_0", "tp_1")
epsilon = 1e-06


def cut_along(x, dim, size):
    before, after = (x.shape[:dim], x.shape[dim + 1 :])
    return jnp.moveaxis(x.reshape(*before, size, -1, *after), dim, 0)


def sum_at_owner(x, axis, dim):
    tiles = cut_along(x, dim, lax.axis_size(axis))
    arrived = lax.all_to_all(tiles, axis, split_axis=0, concat_axis=0, tiled=True)
    return arrived.astype(jnp.float32).sum(axis=0)


def by_axis(x, axes):
    for axis in axes:
        x = lax.psum(x, axis)
    return x


def suffix_sums(failing):
    width = failing.shape[-1]
    pieces = width // width
    shaped = failing.reshape(failing.shape[:-1] + (pieces, width))
    places = jnp.arange(width)
    upper = (places[:, None] > places[None, :]).astype(jnp.float32)
    inner = jnp.matmul(shaped, upper)
    return inner.reshape(failing.shape)


def stick_block(state, queries, keyset, causal):
    outputs, carried = state
    new_out = []
    new_carry = []
    for group in range(2):
        query, stop, scale = queries[group]
        keys = keyset[2 * group]
        values = keyset[2 * group + 1]
        scores = jnp.einsum("qhd,khd->hqk", query, keys, preferred_element_type=jnp.float32)
        scores = scores * scale + jnp.transpose(stop)[:, :, None]
        failing = jax.nn.log_sigmoid(-scores)
        if causal is not None:
            failing = jnp.where(causal, failing, 0.0)
        after = suffix_sums(failing) + carried[group][:, :, None]
        weight = jnp.exp(jax.nn.log_sigmoid(scores) + after)
        if causal is not None:
            weight = jnp.where(causal, weight, 0.0)
        added = jnp.einsum(
            "hqk,khe->qhe", weight.astype(jnp.bfloat16), values, preferred_element_type=jnp.float32
        )
        new_out.append(outputs[group] + added)
        new_carry.append(carried[group] + jnp.sum(failing, axis=-1))
    return (tuple(new_out), tuple(new_carry))


def empty_state(count, heads_a, size_a, heads_b, size_b):
    return (
        (
            jnp.zeros((count, heads_a, size_a), jnp.float32),
            jnp.zeros((count, heads_b, size_b), jnp.float32),
        ),
        (jnp.zeros((heads_a, count), jnp.float32), jnp.zeros((heads_b, count), jnp.float32)),
    )


def joined_rows(state, width_a, width_b):
    count = state[0][0].shape[0]
    return jnp.concatenate(
        [
            state[0][0].astype(jnp.bfloat16).reshape(count, width_a),
            state[0][1].astype(jnp.bfloat16).reshape(count, width_b),
        ],
        axis=1,
    )


def shards(
    query_a,
    key_a,
    value_a,
    query_b,
    key_b,
    value_b,
    stop_a,
    stop_b,
    out_a,
    out_b,
    resid,
    mix_gain,
    ffn_gain,
    routes,
    gates,
    exp_gate,
    exp_up,
    exp_down,
    sh_gate,
    sh_up,
    sh_down,
):
    rows = query_a.shape[0]
    heads_a = stop_a.shape[1]
    heads_b = stop_b.shape[1]
    width_a = query_a.shape[1]
    width_b = query_b.shape[1]
    size_a = width_a // heads_a
    size_b = width_b // heads_b

    def unpack(joined):
        count = joined.shape[0]
        return (
            joined[:, :width_a].reshape(count, heads_a, size_a),
            joined[:, width_a : 2 * width_a].reshape(count, heads_a, size_a),
            joined[:, 2 * width_a : 2 * width_a + width_b].reshape(count, heads_b, size_b),
            joined[:, 2 * width_a + width_b :].reshape(count, heads_b, size_b),
        )

    joined_local = jnp.concatenate([key_a, value_a, key_b, value_b], axis=1)
    places = jnp.arange(rows)
    position = lax.axis_index("sp")
    n_sp = lax.axis_size("sp")
    count = query_a.shape[0]
    queries = (
        (query_a.reshape(count, heads_a, size_a), stop_a, size_a ** (-0.5)),
        (query_b.reshape(count, heads_b, size_b), stop_b, size_b ** (-0.5)),
    )
    causal = (places[None, :] < places[:, None])[None]
    state = stick_block(
        empty_state(rows, heads_a, size_a, heads_b, size_b), queries, unpack(joined_local), causal
    )
    gathered = lax.all_gather(joined_local, "sp", axis=0, tiled=True)

    def turn(step, inner_state):
        start = jnp.maximum(position - step, 0) * rows
        piece = lax.dynamic_slice_in_dim(gathered, start, rows, 0)
        return lax.cond(
            position >= step,
            lambda inputs: stick_block(inputs, queries, unpack(piece), None),
            lambda inputs: inputs,
            inner_state,
        )

    state = lax.fori_loop(1, n_sp, turn, state)
    attended = joined_rows(state, width_a, width_b)
    attended_a = attended[:, :width_a]
    attended_b = attended[:, width_a:]
    partial_value = jnp.dot(attended_a, out_a, preferred_element_type=jnp.float32)
    partial_value = partial_value + jnp.dot(attended_b, out_b, preferred_element_type=jnp.float32)
    mixed = sum_at_owner(partial_value.astype(jnp.bfloat16), TP, 1)
    mix_total = by_axis(jnp.sum(mixed * mixed, axis=1), TP)
    branch = mixed * lax.rsqrt(mix_total / D + epsilon)[:, None] * mix_gain[None, :]
    stream = lax.optimization_barrier((resid.astype(jnp.float32) + branch).astype(jnp.bfloat16))
    stream_f = stream.astype(jnp.float32)
    ffn_total = by_axis(jnp.sum(stream_f * stream_f, axis=1), TP)
    normed = (stream_f * lax.rsqrt(ffn_total / D + epsilon)[:, None] * ffn_gain[None, :]).astype(
        jnp.bfloat16
    )
    shared_gate, shared_up = (
        lax.psum(
            jnp.dot(normed, sh_gate, preferred_element_type=jnp.float32).astype(jnp.bfloat16), TP
        ).astype(jnp.float32),
        lax.psum(
            jnp.dot(normed, sh_up, preferred_element_type=jnp.float32).astype(jnp.bfloat16), TP
        ).astype(jnp.float32),
    )
    shared_hidden = (jax.nn.silu(shared_gate) * shared_up).astype(jnp.bfloat16)
    shared_out = jnp.dot(shared_hidden, sh_down, preferred_element_type=jnp.float32)
    local_experts = exp_gate.shape[0]
    experts = local_experts * n_sp
    top_count = routes.shape[1]
    capacity = max(1, (3 * rows * top_count + 2 * experts - 1) // (2 * experts))
    flat_routes = routes.reshape(-1)
    onehot = (flat_routes[:, None] == jnp.arange(experts, dtype=jnp.int32)[None, :]).astype(
        jnp.int32
    )
    earlier = jnp.cumsum(onehot, axis=0) - onehot
    slot = flat_routes * capacity + jnp.sum(earlier * onehot, axis=1)
    chooser = (slot[:, None] == jnp.arange(experts * capacity, dtype=jnp.int32)[None, :]).astype(
        jnp.bfloat16
    )
    chooser = jnp.sum(chooser.reshape(rows, top_count, experts * capacity), axis=1)
    outgoing = jnp.einsum("rs,rc->sc", chooser, normed, preferred_element_type=jnp.float32).astype(
        jnp.bfloat16
    )
    outgoing = outgoing.reshape(n_sp, local_experts, capacity, normed.shape[1])
    arrived = lax.all_to_all(outgoing, "sp", split_axis=0, concat_axis=0, tiled=True)
    gate_part = jnp.einsum("segd,edf->segf", arrived, exp_gate, preferred_element_type=jnp.float32)
    up_part = jnp.einsum("segd,edf->segf", arrived, exp_up, preferred_element_type=jnp.float32)
    gate_pre = lax.psum(gate_part.astype(jnp.bfloat16), TP).astype(jnp.float32)
    up_pre = lax.psum(up_part.astype(jnp.bfloat16), TP).astype(jnp.float32)
    hidden = (jax.nn.silu(gate_pre) * up_pre).astype(jnp.bfloat16)
    produced = jnp.einsum("segf,efd->segd", hidden, exp_down, preferred_element_type=jnp.float32)
    returned = lax.all_to_all(
        produced.astype(jnp.bfloat16), "sp", split_axis=0, concat_axis=0, tiled=True
    )
    flat_back = returned.reshape(experts * capacity, returned.shape[3])
    picked = jnp.take(flat_back, slot, axis=0).reshape(rows, top_count, returned.shape[3])
    routed = jnp.sum(gates[:, :, None] * picked.astype(jnp.float32), axis=1)
    moe = routed + shared_out
    result = stream_f + moe
    return result.astype(jnp.bfloat16)


def solution(mesh):
    finer = Mesh(mesh.devices.reshape(mesh.shape["sp"], 4, 4), ("sp", "tp_0", "tp_1"))
    in_specs = (
        P("sp", TP),
        P("sp", TP),
        P("sp", TP),
        P("sp", TP),
        P("sp", TP),
        P("sp", TP),
        P("sp", TP),
        P("sp", TP),
        P(TP, None),
        P(TP, None),
        P("sp", TP),
        P(TP),
        P(TP),
        P("sp", None),
        P("sp", None),
        P("sp", TP, None),
        P("sp", TP, None),
        P("sp", None, TP),
        P(TP, None),
        P(TP, None),
        P(None, TP),
    )
    out_specs = P("sp", TP)
    return jax.shard_map(
        shards, mesh=finer, in_specs=in_specs, out_specs=out_specs, check_vma=False
    )
```

profile of v0, /device:TPU:1, one launch (start us, length us, event | category | flops | bytes accessed | tf_op | source)
XLA Modules:
  0.0 487.4 jit_solution(6028487693172046048)
XLA Ops:
  6.5 1.6 pad_maximum_fusion
  8.2 0.9 copy.128
  9.1 0.9 copy.131
  10.0 0.9 copy.127
  10.9 0.8 copy.137
  12.0 1.1 fusion.127
  13.2 0.5 fusion.75
  13.7 0.3 fusion.133
  14.0 0.3 fusion.98
  14.3 0.2 fusion.99
  14.5 0.8 fusion.73
  15.3 76.1 %all-gather.2.cloned.1.call-done = bf16[6144,512]{1,0:T(8,128)(2,1)} async-done(((bf16[192,512]{1,0:T(8,128)(2,1)}), bf16[6144,512]{1,0:T(8,128)(2,1)}) %all-gather.2.cloned.1.call-update) | async-done | bytes 6291472 | tf_op jit(solution)/shard_map/all_gather | solution.py:138
  91.4 8.7 %copy.134 = bf16[6144,512]{0,1:T(8,128)(2,1)} copy(bf16[6144,512]{1,0:T(8,128)(2,1)} %all-gather.2.cloned.1.call-done) | data formatting | bytes 12582912 | tf_op jit(solution)/shard_map/while | solution.py:150
  100.1 6.4 %while.19 = (s32[]{:T(128)}, f32[192,2,64]{0,2,1:T(8,128)S(1)}, f32[192,1,128]{2,0,1:T(8,128)S(1)}, f32[2,192]{1,0:T(2,128)S(1)}, f32[1,192]{1,0:T(1,128)S(1)}, ...) while((s32[]{:T(128)}, f32[192,2,64]{0,2,1:T(8,128)S(1)}, ...), condition=%wide.region_7.8_spmd, body=%wide.region_2.7_spmd.sunk | while | flops 83325512 | bytes 2064037 | solution.py:150
  100.1 5.1 %conditional.2 = ((f32[192,2,64]{0,2,1:T(8,128)S(1)}, f32[192,1,128]{2,0,1:T(8,128)S(1)}, f32[2,192]{1,0:T(2,128)S(1)}, f32[1,192]{1,0:T(1,128)S(1)})) conditional(s32[]{:T(128)} %convert_element_type.258, (f32[192,2,64]{0,2,1:T(8,128)S(1)}, f32[192,1,128]{2,0,1:T(8,128)S(1)}, f32[2,192]{1,0:T(2,128)S(1)}, f32[1,192]{1,0:T(1,128)S(1)}) %tuple.58, ...), branch_computations={%region_3.3_spmd, %region_4.6_spmd} | conditional | flops 83325512 | bytes 2063786 | solution.py:143
  100.1 1.1 constant_dynamic-slice_fusion
  101.1 0.5 fusion.25
  101.6 0.7 fusion.12
  102.4 1.3 fusion.43
  103.7 1.5 fusion.13
  106.5 0.4 fusion.154
  106.9 0.6 copy-done.1
  107.5 0.4 fusion.60
  107.9 1.1 copy.166
  109.0 6.7 %all-to-all-start = ((bf16[16,192,128]{2,1,0:T(8,128)(2,1)}), bf16[16,192,128]{2,1,0:T(8,128)(2,1)S(1)}, u32[]{:S(2)}, u32[]{:S(2)}) async-start(bf16[16,192,128]{2,1,0:T(8,128)(2,1)} %bitcast.107), calls=%async_computation | async-start | bytes 1572864 | tf_op jit(solution)/shard_map/all_to_all | solution.py:19
  116.0 0.2 fusion.108
  116.6 9.7 %all-to-all-done = bf16[16,192,128]{2,1,0:T(8,128)(2,1)S(1)} async-done(((bf16[16,192,128]{2,1,0:T(8,128)(2,1)}), bf16[16,192,128]{2,1,0:T(8,128)(2,1)S(1)}, u32[]{:S(2)}, u32[]{:S(2)}) %all-to-all-start) | async-done | bytes 786464 | tf_op jit(solution)/shard_map/all_to_all | solution.py:19
  126.6 6.5 %psum.56 = f32[192]{0:T(256)S(1)} all-reduce(f32[192]{0:T(256)S(1)} %multiply_reduce_fusion.1), channel_id=1, replica_groups=mesh['sp'=32,'tp_0'=4,'tp_1'=4] {'tp_0'}, use_global_device_ids=true, to_apply=%region_10.11 | all-reduce | flops 192 | bytes 1536 | tf_op jit(solution)/shard_map/psum | solution.py:25
  133.1 6.8 %psum.57 = f32[192]{0:T(256)S(1)} all-reduce(f32[192]{0:T(256)S(1)} %psum.56), channel_id=1, replica_groups=mesh['sp'=32,'tp_0'=4,'tp_1'=4] {'tp_1'}, use_global_device_ids=true, to_apply=%region_11.12 | all-reduce | flops 192 | bytes 1536 | tf_op jit(solution)/shard_map/psum | solution.py:25
  140.1 6.5 %psum.58 = f32[192]{0:T(256)S(1)} all-reduce(f32[192]{0:T(256)S(1)} %fusion.130), channel_id=1, replica_groups=mesh['sp'=32,'tp_0'=4,'tp_1'=4] {'tp_0'}, use_global_device_ids=true, to_apply=%region_17.18 | all-reduce | flops 192 | bytes 1536 | tf_op jit(solution)/shard_map/psum | solution.py:25
  146.6 7.1 %psum.59 = f32[192]{0:T(256)S(1)} all-reduce(f32[192]{0:T(256)S(1)} %psum.58), channel_id=1, replica_groups=mesh['sp'=32,'tp_0'=4,'tp_1'=4] {'tp_1'}, use_global_device_ids=true, to_apply=%region_18.19 | all-reduce | flops 192 | bytes 1536 | tf_op jit(solution)/shard_map/psum | solution.py:25
  153.7 0.3 convolution_convert_fusion.5
  154.1 0.7 copy.143
  154.9 161.9 %all-to-all-start.1 = ((bf16[32,4,5,128]{3,1,2,0:T(4,128)(2,1)}), bf16[32,4,5,128]{3,1,2,0:T(4,128)(2,1)S(1)}, u32[]{:S(2)}, u32[]{:S(2)}) async-start(bf16[32,4,5,128]{3,1,2,0:T(4,128)(2,1)} %copy.143), calls=%async_computation.1 | async-start | bytes 327680 | tf_op jit(solution)/shard_map/all_to_all | solution.py:193
  316.8 0.9 convolution_convert_fusion.3
  317.7 0.9 convolution_convert_fusion.2
  318.7 15.2 %all-to-all-done.1 = bf16[32,4,5,128]{3,1,2,0:T(4,128)(2,1)S(1)} async-done(((bf16[32,4,5,128]{3,1,2,0:T(4,128)(2,1)}), bf16[32,4,5,128]{3,1,2,0:T(4,128)(2,1)S(1)}, u32[]{:S(2)}, u32[]{:S(2)}) %all-to-all-start.1) | async-done | bytes 163872 | tf_op jit(solution)/shard_map/all_to_all | solution.py:193
  333.9 1.2 fusion.61
  335.0 1.2 fusion.62
  336.2 106.3 %all-reduce.3.cloned.1.call-done = (bf16[32,4,5,512]{3,0,2,1:T(8,128)(2,1)}, bf16[32,4,5,512]{3,0,2,1:T(8,128)(2,1)}, bf16[192,512]{1,0:T(8,128)(2,1)}, bf16[192,512]{1,0:T(8,128)(2,1)}) async-done(((bf16[32,4,5,512]{3,0,2,1:T(8,128)(2,1)}, bf16[32,4,5,512]{3,0,2,1:T(8,128)(2,1)}, bf16[192,512]{1,0:T(8,128)(2,1)}, bf16[192,512]{1,0:T(8,128)(2,1)}), (bf16[32,4,5,512]{3,0,2,1:T(8,128)(2,1)}, ...) | async-done | bytes 1703952 | tf_op jit(solution)/shard_map/psum | solution.py:197
  442.6 1.8 fusion.71
  444.5 0.7 copy.146
  445.2 14.6 %all-to-all-start.2 = ((bf16[32,4,5,128]{3,1,2,0:T(4,128)(2,1)}), bf16[32,4,5,128]{3,1,2,0:T(4,128)(2,1)S(1)}, u32[]{:S(2)}, u32[]{:S(2)}) async-start(bf16[32,4,5,128]{3,1,2,0:T(4,128)(2,1)} %copy.146), calls=%async_computation.2 | async-start | bytes 327680 | tf_op jit(solution)/shard_map/all_to_all | solution.py:200
  460.1 0.2 copy.142
  460.5 16.5 %all-to-all-done.2 = bf16[32,4,5,128]{3,1,2,0:T(4,128)(2,1)S(1)} async-done(((bf16[32,4,5,128]{3,1,2,0:T(4,128)(2,1)}), bf16[32,4,5,128]{3,1,2,0:T(4,128)(2,1)S(1)}, u32[]{:S(2)}, u32[]{:S(2)}) %all-to-all-start.2) | async-done | bytes 163872 | tf_op jit(solution)/shard_map/all_to_all | solution.py:200
  477.1 1.4 gather_fusion
  478.6 1.1 multiply_reduce_fusion
  479.7 0.9 fusion.77
  (102 shorter events, 2.6 us)
Async XLA Ops:
  6.5 100.0 %copy-start = (bf16[128,2048]{1,0:T(8,128)(2,1)S(1)}, bf16[128,2048]{1,0:T(8,128)(2,1)}, u32[]{:S(2)}) copy-start(bf16[128,2048]{1,0:T(8,128)(2,1)} %param.33) | copy-start | bytes 1572868
  6.5 6.6 %copy-start.6 = (bf16[192,128]{1,0:T(8,128)(2,1)S(1)}, bf16[192,128]{1,0:T(8,128)(2,1)}, u32[]{:S(2)}) copy-start(bf16[192,128]{1,0:T(8,128)(2,1)} %param.30) | copy-start | bytes 147460
  6.5 84.8 %all-gather.2.cloned.1.call-start = ((), (), s32[]{:S(2)}) async-start(), calls=%async_computation.3 | async-start | bytes 6488064 | tf_op jit(solution)/shard_map/all_gather | solution.py:138
  8.2 5.5 %copy-start.10 = (f32[192,2]{0,1:T(2,128)S(1)}, f32[192,2]{0,1:T(2,128)}, u32[]{:S(2)}) copy-start(f32[192,2]{0,1:T(2,128)} %param.31) | copy-start | bytes 4612
  15.2 84.8 %copy-start.17 = (bf16[192,128]{1,0:T(8,128)(2,1)S(1)}, bf16[192,128]{1,0:T(8,128)(2,1)}, u32[]{:S(2)}) copy-start(bf16[192,128]{1,0:T(8,128)(2,1)} %param.28) | copy-start | bytes 147460
  15.3 84.8 %copy-start.18 = (f32[192,1]{0,1:T(1,128)S(1)}, f32[192,1]{0,1:T(1,128)}, u32[]{:S(2)}) copy-start(f32[192,1]{0,1:T(1,128)} %param.32) | copy-start | bytes 2308
  106.5 1.0 copy-start.1
  109.0 7.4 %copy-start.8 = (s32[192,2]{0,1:T(2,128)S(1)}, s32[192,2]{0,1:T(2,128)}, u32[]{:S(2)}) copy-start(s32[192,2]{0,1:T(2,128)} %param.38) | copy-start | bytes 4612
  109.0 17.3 %all-to-all-start = ((bf16[16,192,128]{2,1,0:T(8,128)(2,1)}), bf16[16,192,128]{2,1,0:T(8,128)(2,1)S(1)}, u32[]{:S(2)}, u32[]{:S(2)}) async-start(bf16[16,192,128]{2,1,0:T(8,128)(2,1)} %bitcast.107), calls=%async_computation | async-start | bytes 1572864 | tf_op jit(solution)/shard_map/all_to_all | solution.py:19
  115.7 24.2 %copy-start.7 = (bf16[192,128]{1,0:T(8,128)(2,1)S(1)}, bf16[192,128]{1,0:T(8,128)(2,1)}, u32[]{:S(2)}) copy-start(bf16[192,128]{1,0:T(8,128)(2,1)} %param.35) | copy-start | bytes 147460
  115.7 24.2 %copy-start.12 = (f32[128]{0:T(128)S(1)}, f32[128]{0:T(128)}, u32[]{:S(2)}) copy-start(f32[128]{0:T(128)} %param.36) | copy-start | bytes 1540
  115.7 38.0 %copy-start.9 = (f32[128]{0:T(128)S(1)}, f32[128]{0:T(128)}, u32[]{:S(2)}) copy-start(f32[128]{0:T(128)} %param.37) | copy-start | bytes 1540
  116.4 200.3 %copy-start.4 = (bf16[128,512]{1,0:T(8,128)(2,1)S(1)}, bf16[128,512]{1,0:T(8,128)(2,1)}, u32[]{:S(2)}) copy-start(bf16[128,512]{1,0:T(8,128)(2,1)} %param.43) | copy-start | bytes 393220
  116.6 201.1 %copy-start.5 = (bf16[128,512]{1,0:T(8,128)(2,1)S(1)}, bf16[128,512]{1,0:T(8,128)(2,1)}, u32[]{:S(2)}) copy-start(bf16[128,512]{1,0:T(8,128)(2,1)} %param.44) | copy-start | bytes 393220
  126.4 207.4 %copy-start.2 = (bf16[4,128,512]{2,1,0:T(8,128)(2,1)S(1)}, bf16[4,128,512]{2,1,0:T(8,128)(2,1)}, u32[]{:S(2)}) copy-start(bf16[4,128,512]{2,1,0:T(8,128)(2,1)} %param.40) | copy-start | bytes 1572868
  154.0 181.0 %copy-start.3 = (bf16[4,128,512]{2,1,0:T(8,128)(2,1)S(1)}, bf16[4,128,512]{2,1,0:T(8,128)(2,1)}, u32[]{:S(2)}) copy-start(bf16[4,128,512]{2,1,0:T(8,128)(2,1)} %param.41) | copy-start | bytes 1572868
  154.9 179.0 %all-to-all-start.1 = ((bf16[32,4,5,128]{3,1,2,0:T(4,128)(2,1)}), bf16[32,4,5,128]{3,1,2,0:T(4,128)(2,1)S(1)}, u32[]{:S(2)}, u32[]{:S(2)}) async-start(bf16[32,4,5,128]{3,1,2,0:T(4,128)(2,1)} %copy.143), calls=%async_computation.1 | async-start | bytes 327680 | tf_op jit(solution)/shard_map/all_to_all | solution.py:193
  316.7 125.9 %all-reduce.3.cloned.1.call-start = ((), (), s32[]{:S(2)}) async-start(), calls=%async_computation.4 | async-start | bytes 3407872 | tf_op jit(solution)/shard_map/psum | solution.py:197
  335.0 107.6 %copy-start.13 = (bf16[4,512,128]{2,1,0:T(8,128)(2,1)S(1)}, bf16[4,512,128]{2,1,0:T(8,128)(2,1)}, u32[]{:S(2)}) copy-start(bf16[4,512,128]{2,1,0:T(8,128)(2,1)} %param.42) | copy-start | bytes 1572868
  442.6 17.7 %copy-start.11 = (f32[192,2]{0,1:T(2,128)S(1)}, f32[192,2]{0,1:T(2,128)}, u32[]{:S(2)}) copy-start(f32[192,2]{0,1:T(2,128)} %param.39) | copy-start | bytes 4612
  444.4 35.2 %copy-start.14 = (bf16[192,512]{1,0:T(8,128)(2,1)S(1)}, bf16[192,512]{1,0:T(8,128)(2,1)}, u32[]{:S(2)}) copy-start(bf16[192,512]{1,0:T(8,128)(2,1)} %get-tuple-element.401) | copy-start | bytes 589828
  444.5 35.2 %copy-start.15 = (bf16[192,512]{1,0:T(8,128)(2,1)S(1)}, bf16[192,512]{1,0:T(8,128)(2,1)}, u32[]{:S(2)}) copy-start(bf16[192,512]{1,0:T(8,128)(2,1)} %get-tuple-element.402) | copy-start | bytes 589828
  444.5 35.2 %copy-start.16 = (bf16[512,128]{1,0:T(8,128)(2,1)S(1)}, bf16[512,128]{1,0:T(8,128)(2,1)}, u32[]{:S(2)}) copy-start(bf16[512,128]{1,0:T(8,128)(2,1)} %param.45) | copy-start | bytes 393220
  445.2 31.7 %all-to-all-start.2 = ((bf16[32,4,5,128]{3,1,2,0:T(4,128)(2,1)}), bf16[32,4,5,128]{3,1,2,0:T(4,128)(2,1)S(1)}, u32[]{:S(2)}, u32[]{:S(2)}) async-start(bf16[32,4,5,128]{3,1,2,0:T(4,128)(2,1)} %copy.146), calls=%async_computation.2 | async-start | bytes 327680 | tf_op jit(solution)/shard_map/all_to_all | solution.py:200
Sparse Core Ops, SparseCore 0:
  9.5 81.8 all-gather.1
  336.4 106.1 all-reduce.2
where the time goes:
time: 491 us; the launch traced here: 487 us
  waiting for transfers between devices  224 us (46%)
  starting transfers between devices  183 us (37%)
  blocking collectives  26.9 us (5%)
  local copies, waits for them, and re-layouts  19.3 us (4%)
  matrix products  14.7 us (3%)
  between operations  13.9 us (3%)
    all_to_all x1, starting transfers between devices, shards(): lax.all_to_all(outgoing, 'sp', split_axis=0, concat_axis=0, tiled=True)  162 us
    psum x1, waiting for transfers between devices, shards(): up_pre = lax.psum(up_part.astype(jnp.bfloat16), TP).astype(jnp.float32)  106 us
    all_gather x1, waiting for transfers between devices, shards(): gathered = lax.all_gather(joined_local, 'sp', axis=0, tiled=True)  76.1 us
    psum x4, blocking collectives, by_axis(): x = lax.psum(x, axis)  26.9 us
    all_to_all x1, waiting for transfers between devices, shards(): lax.all_to_all(produced.astype(jnp.bfloat16), 'sp', split_axis=0, concat_...  16.5 us
    all_to_all x1, waiting for transfers between devices, shards(): lax.all_to_all(outgoing, 'sp', split_axis=0, concat_axis=0, tiled=True)  15.2 us
    all_to_all x1, starting transfers between devices, shards(): lax.all_to_all(produced.astype(jnp.bfloat16), 'sp', split_axis=0, concat_...  14.6 us
  transfers between devices with their start and end apart: 5, of which 5 were waited for; matrix products, arithmetic and copies ran while one was open for 2% of the time, Pallas kernels for 0%

commit v1 on v0

--- a/solution.py
+++ b/solution.py
@@ -7,6 +7,18 @@
 D = 2048
 TP = ("tp_0", "tp_1")
 epsilon = 1e-06
+
+
+def collect(value, axis, dim):
+    ways, here = (lax.axis_size(axis), lax.axis_index(axis))
+    grown, reach = (value, 1)
+    while reach < ways:
+        theirs = lax.ppermute(grown, axis, [(d, d ^ reach) for d in range(ways)])
+        mine_first = jnp.concatenate([grown, theirs], axis=dim)
+        theirs_first = jnp.concatenate([theirs, grown], axis=dim)
+        grown = jnp.where(here & reach == 0, mine_first, theirs_first)
+        reach = 2 * reach
+    return grown
 
 
 def cut_along(x, dim, size):
@@ -135,7 +147,7 @@
     state = stick_block(
         empty_state(rows, heads_a, size_a, heads_b, size_b), queries, unpack(joined_local), causal
     )
-    gathered = lax.all_gather(joined_local, "sp", axis=0, tiled=True)
+    gathered = collect(joined_local, "sp", 0)
 
     def turn(step, inner_state):
         start = jnp.maximum(position - step, 0) * rows

time: 491 us -> 913 us (1.86)
  waiting for transfers between devices: 224 us -> 525 us
  starting transfers between devices: 183 us -> 300 us
  other arithmetic: 4.28 us -> 17.5 us
    ppermute x0 -> x5, waiting for transfers between devices: none -> 377 us  [collect(): theirs = lax.ppermute(grown, axis, [(d, d ^ reach) for d in range(ways)])]
    all_to_all x1, starting transfers between devices: 6.67 us -> 152 us  [sum_at_owner(): lax.all_to_all(tiles, axis, split_axis=0, concat_axis=0, tiled=True)]
    all_gather x1 -> x0, waiting for transfers between devices: 76.1 us -> none  [shards(): gathered = lax.all_gather(joined_local, 'sp', axis=0, tiled=True)]
    all_to_all x1, starting transfers between devices: 162 us -> 106 us  [shards(): lax.all_to_all(outgoing, 'sp', split_axis=0, concat_axis=0, tiled=True)]
    ppermute x0 -> x5, starting transfers between devices: none -> 26.9 us  [collect(): theirs = lax.ppermute(grown, axis, [(d, d ^ reach) for d in range(ways)])]
    select_n x0 -> x5, other arithmetic: none -> 14.8 us  [collect(): grown = jnp.where(here & reach == 0, mine_first, theirs_first)]
  transfers between devices with their start and end apart: 5 -> 9, of which waited for: 5 -> 9; matrix products, arithmetic and copies ran while one was open for 2% -> 1% of each run, Pallas kernels for 0% -> 0%
where the time goes in v1:
time: 913 us; the launch traced here: 909 us
  waiting for transfers between devices  525 us (58%)
  starting transfers between devices  300 us (33%)
  blocking collectives  26.9 us (3%)
  other arithmetic  17.5 us (2%)
  between operations  14 us (2%)
  matrix products  13.9 us (2%)
  local copies, waits for them, and re-layouts  10.4 us (1%)
    ppermute x5, waiting for transfers between devices, collect(): theirs = lax.ppermute(grown, axis, [(d, d ^ reach) for d in range(ways)])  377 us
    all_to_all x1, starting transfers between devices, sum_at_owner(): lax.all_to_all(tiles, axis, split_axis=0, concat_axis=0, tiled=True)  152 us
    all_to_all x1, starting transfers between devices, shards(): lax.all_to_all(outgoing, 'sp', split_axis=0, concat_axis=0, tiled=True)  106 us
    psum x1, waiting for transfers between devices, shards(): up_pre = lax.psum(up_part.astype(jnp.bfloat16), TP).astype(jnp.float32)  106 us
    ppermute x5, starting transfers between devices, collect(): theirs = lax.ppermute(grown, axis, [(d, d ^ reach) for d in range(ways)])  26.9 us
    psum x4, blocking collectives, by_axis(): x = lax.psum(x, axis)  26.9 us
  transfers between devices with their start and end apart: 9, of which 9 were waited for; matrix products, arithmetic and copies ran while one was open for 1% of the time, Pallas kernels for 0%

profile of v1, /device:TPU:1, one launch (start us, length us, event | category | flops | bytes accessed | tf_op | source)
XLA Modules:
  0.0 909.3 jit_solution(2390480599174362944)
XLA Ops:
  6.5 1.0 copy.137
  7.5 0.9 copy.140
  8.4 0.9 copy.145
  9.3 0.9 copy.146
  10.3 8.7 collective-permute-start
  19.0 1.1 collective-permute-done
  20.5 1.9 collective-permute-start.1
  22.4 10.3 %collective-permute-done.1 = bf16[384,512]{0,1:T(8,128)(2,1)S(1)} collective-permute-done((bf16[384,512]{0,1:T(8,128)(2,1)S(1)}, bf16[384,512]{0,1:T(8,128)(2,1)S(1)}, u32[]{:S(2)}, u32[]{:S(2)}) %collective-permute-start.1) | collective-permute-done | bytes 393248 | tf_op jit(solution)/shard_map/ppermute | solution.py:16
  32.8 1.9 collective-permute-start.2
  34.8 37.3 %collective-permute-done.2 = bf16[768,512]{0,1:T(8,128)(2,1)} collective-permute-done((bf16[768,512]{0,1:T(8,128)(2,1)S(1)}, bf16[768,512]{0,1:T(8,128)(2,1)}, u32[]{:S(2)}, u32[]{:S(2)}) %collective-permute-start.2) | collective-permute-done | bytes 786464 | tf_op jit(solution)/shard_map/ppermute | solution.py:16
  72.0 1.7 maximum_select_fusion.2
  73.8 3.5 collective-permute-start.3
  77.4 204.9 %collective-permute-done.3 = bf16[1536,512]{0,1:T(8,128)(2,1)} collective-permute-done((bf16[1536,512]{0,1:T(8,128)(2,1)S(1)}, bf16[1536,512]{0,1:T(8,128)(2,1)}, u32[]{:S(2)}, u32[]{:S(2)}) %collective-permute-start.3) | collective-permute-done | bytes 1572896 | tf_op jit(solution)/shard_map/ppermute | solution.py:16
  282.2 4.0 maximum_select_fusion.1
  286.2 10.8 %collective-permute-start.4 = (bf16[3072,512]{0,1:T(8,128)(2,1)}, bf16[3072,512]{0,1:T(8,128)(2,1)}, u32[]{:S(2)}, u32[]{:S(2)}) collective-permute-start(bf16[3072,512]{0,1:T(8,128)(2,1)} %maximum_select_fusion.1), channel_id=1, source_target_pairs={{0,256},{16,272},{32,288},{48,304},{64,320},{80,336},{96,352},{112... | collective-permute-start | bytes 9437192 | tf_op jit(solution)/shard_map/ppermute | solution.py:16
  298.0 0.5 fusion.75
  299.3 0.8 fusion.73
  300.0 123.1 %collective-permute-done.4 = bf16[3072,512]{0,1:T(8,128)(2,1)} collective-permute-done((bf16[3072,512]{0,1:T(8,128)(2,1)}, bf16[3072,512]{0,1:T(8,128)(2,1)}, u32[]{:S(2)}, u32[]{:S(2)}) %collective-permute-start.4) | collective-permute-done | bytes 3145760 | tf_op jit(solution)/shard_map/ppermute | solution.py:16
  423.2 8.6 maximum_select_fusion
  431.8 6.5 while.19
  431.8 5.1 conditional.2
  431.8 1.1 constant_dynamic-slice_fusion
  432.9 0.5 fusion.25
  433.4 0.7 fusion.12
  434.1 1.3 fusion.43
  435.4 1.5 fusion.13
  439.1 1.1 copy.178
  440.2 151.7 %all-to-all-start = ((bf16[16,192,128]{2,1,0:T(8,128)(2,1)}), bf16[16,192,128]{2,1,0:T(8,128)(2,1)S(1)}, u32[]{:S(2)}, u32[]{:S(2)}) async-start(bf16[16,192,128]{2,1,0:T(8,128)(2,1)} %bitcast.107), calls=%async_computation | async-start | bytes 1572864 | tf_op jit(solution)/shard_map/all_to_all | solution.py:31
  592.9 10.6 %all-to-all-done = bf16[16,192,128]{2,1,0:T(8,128)(2,1)S(1)} async-done(((bf16[16,192,128]{2,1,0:T(8,128)(2,1)}), bf16[16,192,128]{2,1,0:T(8,128)(2,1)S(1)}, u32[]{:S(2)}, u32[]{:S(2)}) %all-to-all-start) | async-done | bytes 786464 | tf_op jit(solution)/shard_map/all_to_all | solution.py:31
  603.7 6.5 psum.56
  610.2 6.6 psum.57
  617.1 6.6 psum.58
  623.7 7.1 psum.59
  631.3 0.7 copy.155
  632.0 106.5 %all-to-all-start.1 = ((bf16[32,4,5,128]{3,1,2,0:T(4,128)(2,1)}), bf16[32,4,5,128]{3,1,2,0:T(4,128)(2,1)S(1)}, u32[]{:S(2)}, u32[]{:S(2)}) async-start(bf16[32,4,5,128]{3,1,2,0:T(4,128)(2,1)} %copy.155), calls=%async_computation.1 | async-start | bytes 327680 | tf_op jit(solution)/shard_map/all_to_all | solution.py:205
  738.5 0.9 convolution_convert_fusion.3
  739.5 0.9 convolution_convert_fusion.2
  740.4 15.2 %all-to-all-done.1 = bf16[32,4,5,128]{3,1,2,0:T(4,128)(2,1)S(1)} async-done(((bf16[32,4,5,128]{3,1,2,0:T(4,128)(2,1)}), bf16[32,4,5,128]{3,1,2,0:T(4,128)(2,1)S(1)}, u32[]{:S(2)}, u32[]{:S(2)}) %all-to-all-start.1) | async-done | bytes 163872 | tf_op jit(solution)/shard_map/all_to_all | solution.py:205
  755.6 1.2 fusion.61
  756.8 1.2 fusion.62
  758.0 106.4 %all-reduce.3.cloned.1.call-done = (bf16[32,4,5,512]{3,0,2,1:T(8,128)(2,1)}, bf16[32,4,5,512]{3,0,2,1:T(8,128)(2,1)}, bf16[192,512]{1,0:T(8,128)(2,1)}, bf16[192,512]{1,0:T(8,128)(2,1)}) async-done(((bf16[32,4,5,512]{3,0,2,1:T(8,128)(2,1)}, bf16[32,4,5,512]{3,0,2,1:T(8,128)(2,1)}, bf16[192,512]{1,0:T(8,128)(2,1)}, bf16[192,512]{1,0:T(8,128)(2,1)}), (bf16[32,4,5,512]{3,0,2,1:T(8,128)(2,1)}, ...) | async-done | bytes 1703952 | tf_op jit(solution)/shard_map/psum | solution.py:209
  864.4 1.9 fusion.71
  866.3 0.7 copy.158
  867.1 14.6 %all-to-all-start.2 = ((bf16[32,4,5,128]{3,1,2,0:T(4,128)(2,1)}), bf16[32,4,5,128]{3,1,2,0:T(4,128)(2,1)S(1)}, u32[]{:S(2)}, u32[]{:S(2)}) async-start(bf16[32,4,5,128]{3,1,2,0:T(4,128)(2,1)} %copy.158), calls=%async_computation.2 | async-start | bytes 327680 | tf_op jit(solution)/shard_map/all_to_all | solution.py:212
  882.3 16.5 %all-to-all-done.2 = bf16[32,4,5,128]{3,1,2,0:T(4,128)(2,1)S(1)} async-done(((bf16[32,4,5,128]{3,1,2,0:T(4,128)(2,1)}), bf16[32,4,5,128]{3,1,2,0:T(4,128)(2,1)S(1)}, u32[]{:S(2)}, u32[]{:S(2)}) %all-to-all-start.2) | async-done | bytes 163872 | tf_op jit(solution)/shard_map/all_to_all | solution.py:212
  898.9 1.4 gather_fusion
  900.4 1.1 multiply_reduce_fusion
  901.5 0.9 fusion.77
  (119 shorter events, 5.9 us)
Async XLA Ops:
  6.5 431.8 %copy-start = (bf16[128,2048]{1,0:T(8,128)(2,1)S(1)}, bf16[128,2048]{1,0:T(8,128)(2,1)}, u32[]{:S(2)}) copy-start(bf16[128,2048]{1,0:T(8,128)(2,1)} %param.33) | copy-start | bytes 1572868
  10.3 9.9 %collective-permute-start = (bf16[192,512]{0,1:T(8,128)(2,1)S(1)}, bf16[192,512]{0,1:T(8,128)(2,1)S(1)}, u32[]{:S(2)}, u32[]{:S(2)}) collective-permute-start(bf16[192,512]{0,1:T(8,128)(2,1)S(1)} %pad_maximum_fusion), channel_id=1, source_target_pairs={{0,16},{16,0},{32,48},{48,32},{64,80},{80,64},{96,112},{112,96},{1... | collective-permute-start | bytes 589832 | tf_op jit(solution)/shard_map/ppermute | solution.py:16
  20.5 12.2 %collective-permute-start.1 = (bf16[384,512]{0,1:T(8,128)(2,1)S(1)}, bf16[384,512]{0,1:T(8,128)(2,1)S(1)}, u32[]{:S(2)}, u32[]{:S(2)}) collective-permute-start(bf16[384,512]{0,1:T(8,128)(2,1)S(1)} %maximum_select_fusion.4), channel_id=1, source_target_pairs={{0,32},{16,48},{32,0},{48,16},{64,96},{80,112},{96,64},{112,80},{1... | collective-permute-start | bytes 1179656 | tf_op jit(solution)/shard_map/ppermute | solution.py:16
  32.8 39.2 %collective-permute-start.2 = (bf16[768,512]{0,1:T(8,128)(2,1)S(1)}, bf16[768,512]{0,1:T(8,128)(2,1)}, u32[]{:S(2)}, u32[]{:S(2)}) collective-permute-start(bf16[768,512]{0,1:T(8,128)(2,1)S(1)} %maximum_select_fusion.3), channel_id=1, source_target_pairs={{0,64},{16,80},{32,96},{48,112},{64,0},{80,16},{96,32},{112,48},{1... | collective-permute-start | bytes 2359304 | tf_op jit(solution)/shard_map/ppermute | solution.py:16
  73.8 208.5 %collective-permute-start.3 = (bf16[1536,512]{0,1:T(8,128)(2,1)S(1)}, bf16[1536,512]{0,1:T(8,128)(2,1)}, u32[]{:S(2)}, u32[]{:S(2)}) collective-permute-start(bf16[1536,512]{0,1:T(8,128)(2,1)S(1)} %maximum_select_fusion.2), channel_id=1, source_target_pairs={{0,128},{16,144},{32,160},{48,176},{64,192},{80,208},{96,224},{112... | collective-permute-start | bytes 4718600 | tf_op jit(solution)/shard_map/ppermute | solution.py:16
  77.3 219.8 %copy-start.6 = (bf16[192,128]{1,0:T(8,128)(2,1)S(1)}, bf16[192,128]{1,0:T(8,128)(2,1)}, u32[]{:S(2)}) copy-start(bf16[192,128]{1,0:T(8,128)(2,1)} %param.25) | copy-start | bytes 147460
  77.3 219.9 %copy-start.10 = (s32[192,2]{0,1:T(2,128)S(1)}, s32[192,2]{0,1:T(2,128)}, u32[]{:S(2)}) copy-start(s32[192,2]{0,1:T(2,128)} %param.38) | copy-start | bytes 4612
  77.3 220.3 %copy-start.7 = (bf16[192,128]{1,0:T(8,128)(2,1)S(1)}, bf16[192,128]{1,0:T(8,128)(2,1)}, u32[]{:S(2)}) copy-start(bf16[192,128]{1,0:T(8,128)(2,1)} %param.29) | copy-start | bytes 147460
  77.3 220.3 %copy-start.19 = (bf16[192,128]{1,0:T(8,128)(2,1)S(1)}, bf16[192,128]{1,0:T(8,128)(2,1)}, u32[]{:S(2)}) copy-start(bf16[192,128]{1,0:T(8,128)(2,1)} %param.28) | copy-start | bytes 147460
  77.3 220.3 %copy-start.20 = (f32[192,1]{0,1:T(1,128)S(1)}, f32[192,1]{0,1:T(1,128)}, u32[]{:S(2)}) copy-start(f32[192,1]{0,1:T(1,128)} %param.32) | copy-start | bytes 2308
  77.3 220.6 %copy-start.8 = (bf16[192,128]{1,0:T(8,128)(2,1)S(1)}, bf16[192,128]{1,0:T(8,128)(2,1)}, u32[]{:S(2)}) copy-start(bf16[192,128]{1,0:T(8,128)(2,1)} %param.30) | copy-start | bytes 147460
  77.4 221.1 %copy-start.12 = (f32[192,2]{0,1:T(2,128)S(1)}, f32[192,2]{0,1:T(2,128)}, u32[]{:S(2)}) copy-start(f32[192,2]{0,1:T(2,128)} %param.31) | copy-start | bytes 4612
  286.2 136.9 %collective-permute-start.4 = (bf16[3072,512]{0,1:T(8,128)(2,1)}, bf16[3072,512]{0,1:T(8,128)(2,1)}, u32[]{:S(2)}, u32[]{:S(2)}) collective-permute-start(bf16[3072,512]{0,1:T(8,128)(2,1)} %maximum_select_fusion.1), channel_id=1, source_target_pairs={{0,256},{16,272},{32,288},{48,304},{64,320},{80,336},{96,352},{112... | collective-permute-start | bytes 9437192 | tf_op jit(solution)/shard_map/ppermute | solution.py:16
  431.8 6.9 copy-start.1
  439.1 177.8 %copy-start.9 = (bf16[192,128]{1,0:T(8,128)(2,1)S(1)}, bf16[192,128]{1,0:T(8,128)(2,1)}, u32[]{:S(2)}) copy-start(bf16[192,128]{1,0:T(8,128)(2,1)} %param.35) | copy-start | bytes 147460
  439.1 177.8 %copy-start.14 = (f32[128]{0:T(128)S(1)}, f32[128]{0:T(128)}, u32[]{:S(2)}) copy-start(f32[128]{0:T(128)} %param.36) | copy-start | bytes 1540
  439.1 191.7 %copy-start.11 = (f32[128]{0:T(128)S(1)}, f32[128]{0:T(128)}, u32[]{:S(2)}) copy-start(f32[128]{0:T(128)} %param.37) | copy-start | bytes 1540
  440.2 298.3 %copy-start.4 = (bf16[128,512]{1,0:T(8,128)(2,1)S(1)}, bf16[128,512]{1,0:T(8,128)(2,1)}, u32[]{:S(2)}) copy-start(bf16[128,512]{1,0:T(8,128)(2,1)} %param.43) | copy-start | bytes 393220
  440.2 299.3 %copy-start.5 = (bf16[128,512]{1,0:T(8,128)(2,1)S(1)}, bf16[128,512]{1,0:T(8,128)(2,1)}, u32[]{:S(2)}) copy-start(bf16[128,512]{1,0:T(8,128)(2,1)} %param.44) | copy-start | bytes 393220
  440.2 315.4 %copy-start.2 = (bf16[4,128,512]{2,1,0:T(8,128)(2,1)S(1)}, bf16[4,128,512]{2,1,0:T(8,128)(2,1)}, u32[]{:S(2)}) copy-start(bf16[4,128,512]{2,1,0:T(8,128)(2,1)} %param.40) | copy-start | bytes 1572868
  440.2 163.3 %all-to-all-start = ((bf16[16,192,128]{2,1,0:T(8,128)(2,1)}), bf16[16,192,128]{2,1,0:T(8,128)(2,1)S(1)}, u32[]{:S(2)}, u32[]{:S(2)}) async-start(bf16[16,192,128]{2,1,0:T(8,128)(2,1)} %bitcast.107), calls=%async_computation | async-start | bytes 1572864 | tf_op jit(solution)/shard_map/all_to_all | solution.py:31
  592.2 164.6 %copy-start.3 = (bf16[4,128,512]{2,1,0:T(8,128)(2,1)S(1)}, bf16[4,128,512]{2,1,0:T(8,128)(2,1)}, u32[]{:S(2)}) copy-start(bf16[4,128,512]{2,1,0:T(8,128)(2,1)} %param.41) | copy-start | bytes 1572868
  631.2 233.2 %copy-start.15 = (bf16[4,512,128]{2,1,0:T(8,128)(2,1)S(1)}, bf16[4,512,128]{2,1,0:T(8,128)(2,1)}, u32[]{:S(2)}) copy-start(bf16[4,512,128]{2,1,0:T(8,128)(2,1)} %param.42) | copy-start | bytes 1572868
  632.0 123.6 %all-to-all-start.1 = ((bf16[32,4,5,128]{3,1,2,0:T(4,128)(2,1)}), bf16[32,4,5,128]{3,1,2,0:T(4,128)(2,1)S(1)}, u32[]{:S(2)}, u32[]{:S(2)}) async-start(bf16[32,4,5,128]{3,1,2,0:T(4,128)(2,1)} %copy.155), calls=%async_computation.1 | async-start | bytes 327680 | tf_op jit(solution)/shard_map/all_to_all | solution.py:205
  738.5 125.9 %all-reduce.3.cloned.1.call-start = ((), (), s32[]{:S(2)}) async-start(), calls=%async_computation.3 | async-start | bytes 3407872 | tf_op jit(solution)/shard_map/psum | solution.py:209
  864.4 17.7 %copy-start.13 = (f32[192,2]{0,1:T(2,128)S(1)}, f32[192,2]{0,1:T(2,128)}, u32[]{:S(2)}) copy-start(f32[192,2]{0,1:T(2,128)} %param.39) | copy-start | bytes 4612
  864.4 37.1 %copy-start.16 = (bf16[192,512]{1,0:T(8,128)(2,1)S(1)}, bf16[192,512]{1,0:T(8,128)(2,1)}, u32[]{:S(2)}) copy-start(bf16[192,512]{1,0:T(8,128)(2,1)} %get-tuple-element.357) | copy-start | bytes 589828
  864.4 37.1 %copy-start.17 = (bf16[192,512]{1,0:T(8,128)(2,1)S(1)}, bf16[192,512]{1,0:T(8,128)(2,1)}, u32[]{:S(2)}) copy-start(bf16[192,512]{1,0:T(8,128)(2,1)} %get-tuple-element.358) | copy-start | bytes 589828
  864.4 37.1 %copy-start.18 = (bf16[512,128]{1,0:T(8,128)(2,1)S(1)}, bf16[512,128]{1,0:T(8,128)(2,1)}, u32[]{:S(2)}) copy-start(bf16[512,128]{1,0:T(8,128)(2,1)} %param.45) | copy-start | bytes 393220
  867.1 31.7 %all-to-all-start.2 = ((bf16[32,4,5,128]{3,1,2,0:T(4,128)(2,1)}), bf16[32,4,5,128]{3,1,2,0:T(4,128)(2,1)S(1)}, u32[]{:S(2)}, u32[]{:S(2)}) async-start(bf16[32,4,5,128]{3,1,2,0:T(4,128)(2,1)} %copy.158), calls=%async_computation.2 | async-start | bytes 327680 | tf_op jit(solution)/shard_map/all_to_all | solution.py:212
Sparse Core Ops, SparseCore 0:
  758.1 106.2 all-reduce.2
